TPU v7x, 1024 devices: a whole 4x8x16 slice. The times are simulated.
1024 devices in a mesh: ep: 32 (over z, core), tp: 32 (over y, x).
Axes of the slice: x: 4, y: 8, z: 16, core: 2. Of those that a mesh axis runs over, the one named last changes fastest.
Arguments:
- tokens: bfloat16 [8192, 4096], P('ep', 'tp'), may hold values from -2000 to 2000, as said below
- norm_gain: float32 [4096], P('tp'), may hold values from 0.1 to 1.9
- route_ids: int32 [8192, 2], P('ep'), may hold values from 0 to 63, all different within a row; in each aligned block of 256 rows (0 to 255, 256 to 511, ...) at most 10 rows name the same one
- route_gates: float32 [8192, 2], P('ep'), may hold values from 0.1 to 1
- w_gate: bfloat16 [64, 768, 4096], P('ep', None, 'tp'), may hold values from -0.09375 to 0.09375
- w_up: bfloat16 [64, 768, 4096], P('ep', None, 'tp'), may hold values from -0.09375 to 0.09375
- w_down: bfloat16 [64, 768, 4096], P('ep', None, 'tp'), may hold values from -0.21875 to 0.21875
Outputs:
- mixed: bfloat16 [8192, 4096], P('ep', 'tp')
Inputs may be any that keep to these rules, and one draw needn't show every extreme that they name: `route_ids`: each row names 2 different experts; among the 256 rows of one index of ep no expert is named by more than 10 rows, a bound that some block reaches. `tokens`: finite values.
All inputs are finite; a program needn't handle non-finite values.
Results may differ from a plain program's by a relative error of at most 0.025.
Values may be sent and summed in bfloat16 or wider, within the bound.
A program may use at most 32 MiB of HBM per device.

v0:
```python
import jax
import jax.numpy as jnp
from jax import lax
from jax.sharding import PartitionSpec as P

EPSILON = 1e-06


def from_everyone(array, axis):
    copies = jnp.broadcast_to(array, (lax.axis_size(axis), *array.shape))
    return lax.all_to_all(copies, axis, split_axis=0, concat_axis=0, tiled=True)


def taken_together(array, axis):
    return from_everyone(array, axis).sum(axis=0)


def in_blocks(array, dim, length):
    before, after = (array.shape[:dim], array.shape[dim + 1 :])
    return jnp.moveaxis(array.reshape(*before, length, -1, *after), dim, 0)


def sum_at_owner(array, axis, dim):
    parts = in_blocks(array, dim, lax.axis_size(axis))
    arrived = lax.all_to_all(parts, axis, split_axis=0, concat_axis=0, tiled=True)
    return arrived.astype(jnp.float32).sum(axis=0)


def joined_along(parts, dim):
    shape = list(parts.shape[1:])
    shape[dim] *= parts.shape[0]
    return jnp.moveaxis(parts, 0, dim).reshape(shape)


def gathered_copies(array, axis, dim):
    parts = from_everyone(array, axis)
    return joined_along(parts, dim)


def gate_up_term(arrived, gate_w, up_w):
    gate_part = jnp.einsum("rec,efc->ref", arrived, gate_w, preferred_element_type=jnp.float32)
    up_part = jnp.einsum("rec,efc->ref", arrived, up_w, preferred_element_type=jnp.float32)
    return jnp.concatenate([gate_part, up_part], axis=2)


def down_term(down_w, piece):
    return jnp.einsum("ref,efc->rec", piece, down_w, preferred_element_type=jnp.float32)


def activate(owned, hidden_units):
    return (jax.nn.silu(owned[:, :, :hidden_units]) * owned[:, :, hidden_units:]).astype(
        jnp.bfloat16
    )


def shards(tokens, norm_gain, route_ids, route_gates, w_gate, w_up, w_down):
    tok_rows, width_loc = tokens.shape
    top_count = route_ids.shape[1]
    exp_local = w_gate.shape[0]
    hidden_units = w_gate.shape[1]
    n_groups = lax.axis_size("ep")
    n_width = lax.axis_size("tp")
    experts = exp_local * n_groups
    capacity = max(2, (5 * tok_rows * top_count + 4 * experts - 1) // (4 * experts))
    slab_rows = n_groups * capacity
    values = tokens.astype(jnp.float32)
    squares = taken_together(jnp.sum(values * values, axis=1), "tp")
    inverse = lax.rsqrt(squares / (width_loc * n_width) + EPSILON)
    normed = (values * inverse[:, None] * norm_gain[None, :]).astype(jnp.bfloat16)
    flat_ids = route_ids.reshape(-1)
    onehot = (flat_ids[:, None] == jnp.arange(experts, dtype=jnp.int32)[None, :]).astype(jnp.int32)
    before = jnp.cumsum(onehot, axis=0) - onehot
    slot_of = jnp.sum(before * onehot, axis=1)
    target = (flat_ids // exp_local * capacity + slot_of) * exp_local + flat_ids % exp_local
    sources = jnp.repeat(normed, top_count, axis=0)
    buffer = jnp.zeros((slab_rows * exp_local, width_loc), jnp.bfloat16).at[target].set(sources)
    buffer = buffer.reshape(n_groups, capacity, exp_local, width_loc)
    arrived = lax.all_to_all(buffer, "ep", split_axis=0, concat_axis=0, tiled=True).reshape(
        slab_rows, exp_local, width_loc
    )
    owned = sum_at_owner(gate_up_term(arrived, w_gate, w_up).astype(jnp.bfloat16), "tp", 0)
    hidden = activate(owned, hidden_units)
    result = down_term(w_down, gathered_copies(hidden, "tp", 0))
    result = result.astype(jnp.bfloat16).reshape(n_groups, capacity, exp_local, width_loc)
    returned = lax.all_to_all(result, "ep", split_axis=0, concat_axis=0, tiled=True)
    picked = returned.reshape(slab_rows * exp_local, width_loc)[target]
    weighted = (
        picked.astype(jnp.float32).reshape(tok_rows, top_count, width_loc) * route_gates[:, :, None]
    )
    return jnp.sum(weighted, axis=1).astype(jnp.bfloat16)


def solution(mesh):
    placed = (
        P("ep", "tp"),
        P("tp"),
        P("ep", None),
        P("ep", None),
        P("ep", None, "tp"),
        P("ep", None, "tp"),
        P("ep", None, "tp"),
    )
    return jax.shard_map(
        shards, mesh=mesh, in_specs=placed, out_specs=P("ep", "tp"), check_vma=False
    )
```

profile of v0, /device:TPU:1, one launch (start us, length us, event | category | flops | bytes accessed | tf_op | source)
XLA Modules:
  0.0 175.6 jit_solution(16894526453102100478)
XLA Ops:
  0.0 1.0 fusion.7
  1.0 0.6 broadcast_in_dim.9
  1.6 10.5 %all-to-all-start = ((f32[32,1,256]{2,1,0:T(1,128)}), f32[32,1,256]{2,1,0:T(1,128)S(1)}, u32[]{:S(2)}, u32[]{:S(2)}) async-start(f32[32,1,256]{2,1,0:T(1,128)} %broadcast_in_dim.9), calls=%async_computation | async-start | bytes 65536 | tf_op jit(solution)/shard_map/all_to_all | solution.py:11
  12.1 0.8 copy.32
  13.4 1.2 reduce-window.6
  15.1 5.8 %all-to-all-done = f32[32,1,256]{2,1,0:T(1,128)S(1)} async-done(((f32[32,1,256]{2,1,0:T(1,128)}), f32[32,1,256]{2,1,0:T(1,128)S(1)}, u32[]{:S(2)}, u32[]{:S(2)}) %all-to-all-start) | async-done | bytes 32800 | tf_op jit(solution)/shard_map/all_to_all | solution.py:11
  20.9 0.9 fusion.9
  21.9 1.8 %scatter_custom_fusion = bf16[640,128]{1,0:T(8,128)(2,1)S(1)} fusion(s32[512]{0:T(512)S(1)} %bitcast.50, bf16[512,128]{1,0:T(8,128)(2,1)S(1)} %bitcast.48, bf16[]{:T(256)} %constant.38.clone.1), kind=kCustom, calls=%fused_computation.29 | custom fusion | bytes 163842 | tf_op jit(solution)/shard_map/scatter | solution.py:76
  23.7 37.9 %all_to_all.26 = bf16[32,10,2,128]{3,2,1,0:T(2,128)(2,1)S(1)} all-to-all(bf16[32,10,2,128]{3,2,1,0:T(2,128)(2,1)S(1)} %bitcast.46), channel_id=1, replica_groups=mesh['ep'=32,'tp'=32] {'ep'}, dimensions={0} | all-to-all | bytes 327680 | tf_op jit(solution)/shard_map/all_to_all | solution.py:78
  61.7 0.4 fusion
  62.1 1.0 copy.38
  63.2 0.4 fusion.1
  63.6 1.0 copy.40
  64.6 1.7 pad_maximum_fusion
  66.3 48.7 %all_to_all.27 = bf16[32,10,2,1536]{3,2,1,0:T(2,128)(2,1)S(1)} all-to-all(bf16[32,10,2,1536]{3,2,1,0:T(2,128)(2,1)S(1)} %pad_maximum_fusion), channel_id=1, replica_groups=mesh['ep'=32,'tp'=32] {'tp'}, dimensions={0} | all-to-all | bytes 3932160 | tf_op jit(solution)/shard_map/all_to_all | solution.py:25
  114.9 1.6 convert_reduce_fusion
  116.6 0.5 broadcast_in_dim.21
  117.1 29.8 %all_to_all.28 = bf16[32,10,2,768]{3,2,1,0:T(2,128)(2,1)S(1)} all-to-all(bf16[32,10,2,768]{3,2,1,0:T(2,128)(2,1)S(1)} %broadcast_in_dim.21), channel_id=1, replica_groups=mesh['ep'=32,'tp'=32] {'tp'}, dimensions={0} | all-to-all | bytes 1966080 | tf_op jit(solution)/shard_map/all_to_all | solution.py:11
  147.0 0.4 fusion.2
  147.4 0.8 copy.42
  148.2 7.8 %all-to-all-start.4 = ((bf16[32,10,2,128]{3,2,1,0:T(2,128)(2,1)}), bf16[32,10,2,128]{3,2,1,0:T(2,128)(2,1)S(1)}, u32[]{:S(2)}, u32[]{:S(2)}) async-start(bf16[32,10,2,128]{3,2,1,0:T(2,128)(2,1)} %bitcast.12), calls=%async_computation.4 | async-start | bytes 327680 | tf_op jit(solution)/shard_map/all_to_all | solution.py:85
  156.2 17.0 %all-to-all-done.4 = bf16[32,10,2,128]{3,2,1,0:T(2,128)(2,1)S(1)} async-done(((bf16[32,10,2,128]{3,2,1,0:T(2,128)(2,1)}), bf16[32,10,2,128]{3,2,1,0:T(2,128)(2,1)S(1)}, u32[]{:S(2)}, u32[]{:S(2)}) %all-to-all-start.4) | async-done | bytes 163872 | tf_op jit(solution)/shard_map/all_to_all | solution.py:85
  173.2 1.3 gather_fusion
  174.5 1.1 fusion.4
  (23 shorter events, 1.2 us)
Async XLA Ops:
  0.0 61.7 %copy-start = (bf16[2,768,128]{2,1,0:T(8,128)(2,1)S(1)}, bf16[2,768,128]{2,1,0:T(8,128)(2,1)}, u32[]{:S(2)}) copy-start(bf16[2,768,128]{2,1,0:T(8,128)(2,1)} %param.11) | copy-start | bytes 1179652
  1.6 19.2 %all-to-all-start = ((f32[32,1,256]{2,1,0:T(1,128)}), f32[32,1,256]{2,1,0:T(1,128)S(1)}, u32[]{:S(2)}, u32[]{:S(2)}) async-start(f32[32,1,256]{2,1,0:T(1,128)} %broadcast_in_dim.9), calls=%async_computation | async-start | bytes 65536 | tf_op jit(solution)/shard_map/all_to_all | solution.py:11
  21.9 41.2 %copy-start.1 = (bf16[2,768,128]{2,1,0:T(8,128)(2,1)S(1)}, bf16[2,768,128]{2,1,0:T(8,128)(2,1)}, u32[]{:S(2)}) copy-start(bf16[2,768,128]{2,1,0:T(8,128)(2,1)} %param.12) | copy-start | bytes 1179652
  116.5 30.5 %copy-start.3 = (bf16[2,768,128]{2,1,0:T(8,128)(2,1)S(1)}, bf16[2,768,128]{2,1,0:T(8,128)(2,1)}, u32[]{:S(2)}) copy-start(bf16[2,768,128]{2,1,0:T(8,128)(2,1)} %param.13) | copy-start | bytes 1179652
  117.1 38.9 %copy-start.2 = (f32[256,2]{0,1:T(2,128)S(1)}, f32[256,2]{0,1:T(2,128)}, u32[]{:S(2)}) copy-start(f32[256,2]{0,1:T(2,128)} %param.10) | copy-start | bytes 6148
  148.2 25.0 %all-to-all-start.4 = ((bf16[32,10,2,128]{3,2,1,0:T(2,128)(2,1)}), bf16[32,10,2,128]{3,2,1,0:T(2,128)(2,1)S(1)}, u32[]{:S(2)}, u32[]{:S(2)}) async-start(bf16[32,10,2,128]{3,2,1,0:T(2,128)(2,1)} %bitcast.12), calls=%async_computation.4 | async-start | bytes 327680 | tf_op jit(solution)/shard_map/all_to_all | solution.py:85
where the time goes:
time: 177 us; the launch traced here: 176 us
  blocking collectives  116 us (66%)
  waiting for transfers between devices  22.8 us (13%)
  starting transfers between devices  18.3 us (10%)
  local copies, waits for them, and re-layouts  8.82 us (5%)
  other arithmetic  7.81 us (4%)
    all_to_all x1, blocking collectives, sum_at_owner(): lax.all_to_all(parts, axis, split_axis=0, concat_axis=0, tiled=True)  48.7 us
    all_to_all x1, blocking collectives, shards(): lax.all_to_all(buffer, 'ep', split_axis=0, concat_axis=0, tiled=True)  37.9 us
    all_to_all x1, blocking collectives, from_everyone(): return lax.all_to_all(copies, axis, split_axis=0, concat_axis=0, tiled=True)  29.8 us
    all_to_all x1, waiting for transfers between devices, shards(): lax.all_to_all(result, 'ep', split_axis=0, concat_axis=0, tiled=True)  17 us
    all_to_all x1, starting transfers between devices, from_everyone(): return lax.all_to_all(copies, axis, split_axis=0, concat_axis=0, tiled=True)  10.5 us
    all_to_all x1, starting transfers between devices, shards(): lax.all_to_all(result, 'ep', split_axis=0, concat_axis=0, tiled=True)  7.84 us
    all_to_all x1, waiting for transfers between devices, from_everyone(): return lax.all_to_all(copies, axis, split_axis=0, concat_axis=0, tiled=True)  5.79 us
  transfers between devices with their start and end apart: 2, of which 2 were waited for; matrix products, arithmetic and copies ran while one was open for 2% of the time, Pallas kernels for 0%

commit v1 on v0

v1 whole, which is shorter than its diff:
```python
import functools

import jax
import jax.numpy as jnp
from jax import lax
from jax.experimental import pallas as pl
from jax.experimental.pallas import tpu as pltpu
from jax.sharding import PartitionSpec as P

EPSILON = 1e-06
NX = 4
PAD = 16
MESH = pl.DeviceIdType.MESH
F32 = jnp.float32
BF16 = jnp.bfloat16


def dot_nt(a, b):
    return lax.dot_general(a, b, (((1,), (1,)), ((), ())), preferred_element_type=F32)


def dot_nn(a, b):
    return lax.dot_general(a, b, (((1,), (0,)), ((), ())), preferred_element_type=F32)


def kernel(
    n_ep, ny, cap,
    tok_ref, gain_ref, ids_ref, gates_ref, wg_ref, wu_ref, wd_ref,
    out_ref,
    zsend, zrecv, xg, wland, wcat, wdn, gain_all, xs, part, rs, ssq, ssq_all,
    hid, po, xr, back, ret, tcol,
    z_ss, z_rs, r_ss, r_rs, w_ss, w_rs, g_ss, g_rs, x_ss, x_rs,
    y_ss, y_rs, q_ss, q_rs, h_ss, h_rs, o_ss, o_rs, l_sem,
):
    nz = n_ep // 2
    rows = n_ep * PAD
    own = n_ep // ny
    toks = tok_ref.shape[0]
    experts = 2 * n_ep
    half = wg_ref.shape[1] // 2
    feats = tok_ref.shape[1]
    ep = lax.axis_index("ep")
    tp = lax.axis_index("tp")
    z, core = ep // 2, lax.rem(ep, 2)
    y, x = tp // NX, lax.rem(tp, NX)

    def z_peer(i):
        j, c = i // 2, lax.rem(i, 2)
        dz = nz // 2 + (1 - 2 * lax.rem(j, 2)) * ((j + 1) // 2)
        return 2 * lax.rem(z + dz, nz) + c

    def x_peer(k):
        return lax.rem(x + k, NX)

    def y_peer(k):
        return lax.rem(y + k, ny)

    partner = z * 2 + (1 - core)
    x_steps = (2, 1, 3)
    y_steps = sorted(range(1, ny), key=lambda k: -min(k, ny - k))

    barrier = pltpu.get_barrier_semaphore()

    def greet(i, carry):
        pl.semaphore_signal(barrier, inc=1, device_id=(z_peer(i), tp), device_id_type=MESH)
        return carry

    lax.fori_loop(0, 2 * (nz - 1), greet, 0)
    pl.semaphore_signal(barrier, inc=1, device_id=(partner, tp), device_id_type=MESH)
    for k in x_steps:
        pl.semaphore_signal(barrier, inc=1, device_id=(ep, y * NX + x_peer(k)), device_id_type=MESH)
    for k in y_steps:
        pl.semaphore_signal(barrier, inc=1, device_id=(ep, y_peer(k) * NX + x), device_id_type=MESH)

    def w_src(ref, to):
        return ref.at[to // 2, pl.ds(lax.rem(to, 2) * half, half), :]

    own_w = [
        pltpu.make_async_copy(w_src(ref, x), wland.at[n, x], l_sem.at[n])
        for n, ref in enumerate((wg_ref, wu_ref, wd_ref))
    ]
    for copy in own_w:
        copy.start()

    ids = ids_ref[...].astype(F32)
    e_iota = lax.broadcasted_iota(jnp.int32, (experts, toks), 0).astype(F32)
    m0, m1 = e_iota == ids[0:1, :], e_iota == ids[1:2, :]
    named = jnp.where(m0 | m1, 1.0, 0.0).astype(BF16)
    t_row = lax.broadcasted_iota(jnp.int32, (toks, toks), 0)
    t_col = lax.broadcasted_iota(jnp.int32, (toks, toks), 1)
    earlier = jnp.where(t_row < t_col, 1.0, 0.0).astype(BF16)
    before = dot_nn(named, earlier)
    target0 = ids[0:1, :] * PAD + jnp.sum(jnp.where(m0, before, 0.0), axis=0, keepdims=True)
    target1 = ids[1:2, :] * PAD + jnp.sum(jnp.where(m1, before, 0.0), axis=0, keepdims=True)
    chunk = min(256, experts * PAD)
    for n in range(experts * PAD // chunk):
        p_iota = (lax.broadcasted_iota(jnp.int32, (chunk, toks), 0) + n * chunk).astype(F32)
        pick = jnp.where((p_iota == target0) | (p_iota == target1), 1.0, 0.0).astype(BF16)
        block = dot_nn(pick, tok_ref[...]).astype(BF16)
        zsend[pl.ds(n * chunk // PAD, chunk // PAD)] = block.reshape(chunk // PAD, PAD, feats)
    ret[...] = jnp.zeros_like(ret)
    gain_all[x] = gain_ref[...]

    pl.semaphore_wait(barrier, 2 * nz - 1 + (NX - 1) + (ny - 1))

    def z_copy(peer):
        return pltpu.make_async_remote_copy(
            src_ref=zsend.at[pl.ds(2 * peer, 2), pl.ds(0, cap)],
            dst_ref=zrecv.at[:, ep, pl.ds(0, cap)],
            send_sem=z_ss.at[peer], recv_sem=z_rs.at[ep],
            device_id=(peer, tp), device_id_type=MESH,
        )

    def z_arrival(peer):
        return pltpu.make_async_remote_copy(
            src_ref=zsend.at[pl.ds(2 * peer, 2), pl.ds(0, cap)],
            dst_ref=zrecv.at[:, peer, pl.ds(0, cap)],
            send_sem=z_ss.at[peer], recv_sem=z_rs.at[peer],
            device_id=(peer, tp), device_id_type=MESH,
        )

    def each_z(fn):
        def step(i, carry):
            fn(z_peer(i))
            return carry

        lax.fori_loop(0, 2 * (nz - 1), step, 0)
        fn(partner)

    each_z(lambda peer: z_copy(peer).start())

    def w_copy(n, ref, k, slot):
        return pltpu.make_async_remote_copy(
            src_ref=w_src(ref, x_peer(k)), dst_ref=wland.at[n, slot],
            send_sem=w_ss.at[n, k], recv_sem=w_rs.at[n, k],
            device_id=(ep, y * NX + x_peer(k)), device_id_type=MESH,
        )

    def g_copy(k, slot):
        return pltpu.make_async_remote_copy(
            src_ref=gain_ref, dst_ref=gain_all.at[slot],
            send_sem=g_ss.at[k], recv_sem=g_rs.at[k],
            device_id=(ep, y * NX + x_peer(k)), device_id_type=MESH,
        )

    weights = list(enumerate((wg_ref, wu_ref, wd_ref)))
    for k in x_steps:
        g_copy(k, x).start()
    for n, ref in weights:
        for k in x_steps:
            w_copy(n, ref, k, x).start()

    zrecv[0, ep] = zsend[2 * ep]
    zrecv[1, ep] = zsend[2 * ep + 1]

    pad_rows = jnp.zeros((124, toks), F32)
    tcol[...] = jnp.concatenate([target0, target1, gates_ref[...], pad_rows], axis=0).T

    each_z(lambda peer: z_arrival(peer).wait_recv())

    def x_copy(k, slot):
        to = x_peer(k)
        return pltpu.make_async_remote_copy(
            src_ref=zrecv.at[to // 2, :, pl.ds(0, cap)], dst_ref=xg.at[slot, :, pl.ds(0, cap)],
            send_sem=x_ss.at[k], recv_sem=x_rs.at[k],
            device_id=(ep, y * NX + to), device_id_type=MESH,
        )

    for k in x_steps:
        x_copy(k, x).start()
    xg[x] = zrecv[x // 2]

    def came(k):
        return lax.rem(x + NX - k, NX)

    for copy in own_w:
        copy.wait()
    for k in x_steps:
        g_copy(k, came(k)).wait_recv()
        for n, ref in weights:
            w_copy(n, ref, k, came(k)).wait_recv()
    for s in range(NX):
        wcat[0:half, s * feats : (s + 1) * feats] = wland[0, s]
        wcat[half : 2 * half, s * feats : (s + 1) * feats] = wland[1, s]
        wdn[:, s * feats : (s + 1) * feats] = wland[2, s]

    for k in x_steps:
        x_copy(k, came(k)).wait_recv()

    squares = jnp.zeros((rows, feats), F32)
    for s in range(NX):
        raw = xg[s].reshape(rows, feats).astype(F32)
        squares += raw * raw
        xs[:, s * feats : (s + 1) * feats] = (raw * gain_all[s]).astype(BF16)
    sums = jnp.sum(squares, axis=1, keepdims=True)
    lane = lax.broadcasted_iota(jnp.int32, (rows, 128), 1)
    row = lax.broadcasted_iota(jnp.int32, (rows, 128), 0)
    spread = jnp.where(lane == lax.rem(row, 128), sums, 0.0)
    groups = max(1, rows // 128)
    ssq[...] = jnp.concatenate(
        [jnp.sum(spread[g * 128 : (g + 1) * 128], axis=0, keepdims=True) for g in range(groups)], axis=0
    )

    def y_copy(k, slot):
        to = y_peer(k)
        return pltpu.make_async_remote_copy(
            src_ref=part.at[pl.ds(own * to, own), :, pl.ds(0, cap)], dst_ref=rs.at[slot, :, :, pl.ds(0, cap)],
            send_sem=y_ss.at[k], recv_sem=y_rs.at[k],
            device_id=(ep, to * NX + x), device_id_type=MESH,
        )

    def q_copy(k, slot):
        return pltpu.make_async_remote_copy(
            src_ref=ssq, dst_ref=ssq_all.at[slot],
            send_sem=q_ss.at[k], recv_sem=q_rs.at[k],
            device_id=(ep, y_peer(k) * NX + x), device_id_type=MESH,
        )

    for k in y_steps:
        q_copy(k, y).start()
    blocks = max(1, rows // 128)
    per = rows // blocks

    def gate_up(b, carry):
        at = pl.multiple_of(b * per, per)
        both = dot_nt(xs[pl.ds(at, per), :], wcat[...]).astype(BF16)
        for c in range(2 * half // 128):
            part[pl.ds(b * (per // PAD), per // PAD), c] = both[:, c * 128 : (c + 1) * 128].reshape(
                per // PAD, PAD, 128
            )
        return carry

    lax.fori_loop(0, blocks, gate_up, 0)
    for k in y_steps:
        y_copy(k, y).start()

    ssq_all[y] = ssq[...]

    def y_came(k):
        return lax.rem(y + ny - k, ny)

    for k in y_steps:
        q_copy(k, y_came(k)).wait_recv()
    stats = jnp.sum(ssq_all[...], axis=0)
    mine = own * PAD
    lane = lax.broadcasted_iota(jnp.int32, (mine, 128), 1)
    row = lax.broadcasted_iota(jnp.int32, (mine, 128), 0) + y * mine
    picked = jnp.zeros((mine, 128), F32)
    for g in range(groups):
        picked += jnp.where(row == lane + g * 128, stats[g : g + 1, :], 0.0)
    mean = jnp.sum(picked, axis=1, keepdims=True) / (feats * NX * ny)
    inverse = lax.rsqrt(mean + EPSILON)

    for k in y_steps:
        y_copy(k, y_came(k)).wait_recv()

    def summed(c):
        total = part[pl.ds(own * y, own), c].reshape(mine, 128).astype(F32)
        for k in range(1, ny):
            total += rs[y_came(k), :, c].reshape(mine, 128).astype(F32)
        return total * inverse

    tiles = half // 128
    for c in range(tiles):
        gate_act, up_act = summed(c), summed(tiles + c)
        hidden = (gate_act / (1.0 + jnp.exp(-gate_act)) * up_act).astype(BF16)
        hid[pl.ds(own * y, own), c] = hidden.reshape(own, PAD, 128)

    def h_copy(k, slot):
        return pltpu.make_async_remote_copy(
            src_ref=hid.at[pl.ds(own * slot, own), :, pl.ds(0, cap)],
            dst_ref=hid.at[pl.ds(own * slot, own), :, pl.ds(0, cap)],
            send_sem=h_ss.at[k], recv_sem=h_rs.at[k],
            device_id=(ep, y_peer(k) * NX + x), device_id_type=MESH,
        )

    for k in y_steps:
        h_copy(k, y).start()
    for k in y_steps:
        h_copy(k, y_came(k)).wait_recv()

    def down(b, carry):
        held = jnp.concatenate(
            [hid[pl.ds(b * (per // PAD), per // PAD), c].reshape(per, 128) for c in range(tiles)], axis=1
        )
        piece = dot_nn(held, wdn[...]).astype(BF16)
        for s in range(NX):
            po[s, pl.ds(b * (per // PAD), per // PAD)] = piece[:, s * feats : (s + 1) * feats].reshape(
                per // PAD, PAD, feats
            )
        return carry

    lax.fori_loop(0, blocks, down, 0)

    def o_copy(k, slot):
        return pltpu.make_async_remote_copy(
            src_ref=po.at[x_peer(k), :, pl.ds(0, cap)], dst_ref=xr.at[slot, :, pl.ds(0, cap)],
            send_sem=o_ss.at[k], recv_sem=o_rs.at[k],
            device_id=(ep, y * NX + x_peer(k)), device_id_type=MESH,
        )

    for k in x_steps:
        o_copy(k, x).start()
    xr[x] = po[x]
    for k in x_steps:
        o_copy(k, came(k)).wait_recv()
    for e in range(2):
        back[e] = (xr[2 * e].astype(F32) + xr[2 * e + 1].astype(F32)).astype(BF16)

    def r_copy(peer, slot):
        return pltpu.make_async_remote_copy(
            src_ref=back.at[:, peer, pl.ds(0, cap)],
            dst_ref=ret.at[pl.ds(2 * slot, 2), pl.ds(0, cap)],
            send_sem=r_ss.at[peer], recv_sem=r_rs.at[slot],
            device_id=(peer, tp), device_id_type=MESH,
        )

    each_z(lambda peer: r_copy(peer, ep).start())
    for e in range(2):
        ret[2 * ep + e, 0:cap] = back[e, ep, 0:cap]
    each_z(lambda peer: r_copy(peer, peer).wait_recv())

    answers = ret[...].reshape(experts * PAD, feats)
    p_iota = lax.broadcasted_iota(jnp.int32, (toks, experts * PAD), 1).astype(F32)
    mixed = jnp.zeros((toks, feats), F32)
    for k in range(2):
        pick = jnp.where(p_iota == tcol[:, k : k + 1], 1.0, 0.0).astype(BF16)
        mixed += dot_nn(pick, answers) * tcol[:, 2 + k : 3 + k]
    out_ref[...] = mixed.astype(BF16)

    each_z(lambda peer: z_copy(peer).wait_send())
    each_z(lambda peer: r_copy(peer, ep).wait_send())
    for k in x_steps:
        g_copy(k, x).wait_send()
        for n, ref in weights:
            w_copy(n, ref, k, x).wait_send()
        x_copy(k, x).wait_send()
        o_copy(k, x).wait_send()
    for k in y_steps:
        q_copy(k, y).wait_send()
        y_copy(k, y).wait_send()
        h_copy(k, y).wait_send()


def layer(n_ep, n_tp, tokens, norm_gain, route_ids, route_gates, w_gate, w_up, w_down):
    toks, feats = tokens.shape
    ny = n_tp // NX
    experts = 2 * n_ep
    cap = max(2, (5 * toks * 2 + 4 * experts - 1) // (4 * experts))
    half = w_gate.shape[1] // 2
    own = n_ep // ny
    rows = n_ep * PAD
    groups = max(1, rows // 128)
    dma = pltpu.SemaphoreType.DMA
    vmem = pl.BlockSpec(memory_space=pltpu.VMEM)
    hbm = pl.BlockSpec(memory_space=pl.ANY)
    return pl.pallas_call(
        functools.partial(kernel, n_ep, ny, cap),
        out_shape=jax.ShapeDtypeStruct((toks, feats), BF16),
        in_specs=[vmem, vmem, vmem, vmem, hbm, hbm, hbm],
        out_specs=vmem,
        scratch_shapes=[
            pltpu.VMEM((experts, PAD, feats), BF16),
            pltpu.VMEM((2, n_ep, PAD, feats), BF16),
            pltpu.VMEM((NX, n_ep, PAD, feats), BF16),
            pltpu.VMEM((3, NX, half, feats), BF16),
            pltpu.VMEM((2 * half, NX * feats), BF16),
            pltpu.VMEM((half, NX * feats), BF16),
            pltpu.VMEM((NX, 1, feats), F32),
            pltpu.VMEM((rows, NX * feats), BF16),
            pltpu.VMEM((n_ep, 2 * half // 128, PAD, 128), BF16),
            pltpu.VMEM((ny, own, 2 * half // 128, PAD, 128), BF16),
            pltpu.VMEM((groups, 128), F32),
            pltpu.VMEM((ny, groups, 128), F32),
            pltpu.VMEM((n_ep, half // 128, PAD, 128), BF16),
            pltpu.VMEM((NX, n_ep, PAD, feats), BF16),
            pltpu.VMEM((NX, n_ep, PAD, feats), BF16),
            pltpu.VMEM((2, n_ep, PAD, feats), BF16),
            pltpu.VMEM((experts, PAD, feats), BF16),
            pltpu.VMEM((toks, 128), F32),
            dma((n_ep,)), dma((n_ep,)), dma((n_ep,)), dma((n_ep,)),
            dma((3, NX)), dma((3, NX)), dma((NX,)), dma((NX,)), dma((NX,)), dma((NX,)),
            dma((ny,)), dma((ny,)), dma((ny,)), dma((ny,)), dma((ny,)), dma((ny,)),
            dma((NX,)), dma((NX,)), dma((3,)),
        ],
        compiler_params=pltpu.CompilerParams(collective_id=0, has_side_effects=True),
        name="routed_layer",
    )(tokens, norm_gain.reshape(1, feats), route_ids.T, route_gates.T, w_gate, w_up, w_down)


def solution(mesh):
    placed = (
        P("ep", "tp"),
        P("tp"),
        P("ep", None),
        P("ep", None),
        P("ep", None, "tp"),
        P("ep", None, "tp"),
        P("ep", None, "tp"),
    )
    body = functools.partial(layer, mesh.shape["ep"], mesh.shape["tp"])
    return jax.shard_map(body, mesh=mesh, in_specs=placed, out_specs=P("ep", "tp"), check_vma=False)
```

time: 177 us -> 86.5 us (0.49)
  blocking collectives: 116 us -> 0 us
  Pallas kernels: 0 us -> 84.8 us
  waiting for transfers between devices: 22.8 us -> 0 us
  starting transfers between devices: 18.3 us -> 0 us
  other arithmetic: 7.81 us -> 0 us
  local copies, waits for them, and re-layouts: 8.82 us -> 1.47 us
    all_to_all x3 -> x0, blocking collectives: 116 us -> none  [the longest x1 48.7 us: sum_at_owner(): lax.all_to_all(parts, axis, split_axis=0, concat_axis=0, tiled=True)]
    pallas_call x0 -> x1, Pallas kernels: none -> 84.8 us  [layer(): pl.pallas_call(functools.partial(kernel, n_ep, ny, cap), out_shape=jax.Sh...]
    all_to_all x2 -> x0, waiting for transfers between devices: 22.8 us -> none  [the longest x1 17 us: shards(): lax.all_to_all(result, 'ep', split_axis=0, concat_axis=0, tiled=True)]
    all_to_all x2 -> x0, starting transfers between devices: 18.3 us -> none  [the longest x1 10.5 us: from_everyone(): return lax.all_to_all(copies, axis, split_axis=0, concat_axis=0, tiled=True)]
    reduce_sum x5 -> x0, other arithmetic: 3.81 us -> none  [the longest x1 1.57 us: sum_at_owner(): return arrived.astype(jnp.float32).sum(axis=0)]
    transpose x2 -> x0, local copies, waits for them, and re-layouts: 2.03 us -> none  [the longest x1 1.01 us: gate_up_term(): jnp.einsum('rec,efc->ref', arrived, gate_w, preferred_element_type=jnp.fl...]
    scatter x1 -> x0, local copies, waits for them, and re-layouts: 1.79 us -> none  [shards(): jnp.zeros((slab_rows * exp_local, width_loc), jnp.bfloat16).at[target]]
  transfers between devices with their start and end apart: 2 -> 0, of which waited for: 2 -> 0; matrix products, arithmetic and copies ran while one was open for 2% -> 0% of each run, Pallas kernels for 0% -> 0%
where the time goes in v1:
time: 86.5 us; the launch traced here: 86.3 us
  Pallas kernels  84.8 us (98%)
  local copies, waits for them, and re-layouts  1.47 us (2%)
    pallas_call x1, Pallas kernels, layer(): pl.pallas_call(functools.partial(kernel, n_ep, ny, cap), out_shape=jax.Sh...  84.8 us

profile of v1, /device:TPU:1, one launch (start us, length us, event | category | flops | bytes accessed | tf_op | source)
XLA Modules:
  0.0 86.3 jit_solution(7886130208605300973)
XLA Ops:
  0.0 84.8 %routed_layer.1 = bf16[256,128]{1,0:T(8,128)(2,1)} custom-call(bf16[256,128]{1,0:T(8,128)(2,1)} %tok_ref.1, f32[1,128]{1,0:T(1,128)} %bitcast.5, s32[2,256]{1,0:T(2,128)} %bitcast.3, f32[2,256]{1,0:T(2,128)} %bitcast.4, bf16[2,768,128]{2,1,0:T(8,128)(2,1)} %wg_ref.1, bf16[2,768,128]{2,1,0:T(8,128)(2,1)} %wu_ref.1, bf16[2,768,128]{2,1,0:T(8,128)(2,1)} %wd_ref.1), custom_call_target="tpu_custom_call" | custom-call | tf_op jit(solution)/shard_map/routed_layer/pallas_call | solution.py:357
  84.8 1.5 %copy.9 = bf16[256,128]{1,0:T(8,128)(2,1)} copy(bf16[256,128]{1,0:T(8,128)(2,1)} %routed_layer.1) | data formatting | bytes 131072

commit v2 on v1

v2 whole, which is shorter than its diff:
```python
import functools

import jax
import jax.numpy as jnp
from jax import lax
from jax.experimental import pallas as pl
from jax.experimental.pallas import tpu as pltpu
from jax.sharding import PartitionSpec as P

EPSILON = 1e-06
NX = 4
PAD = 16
CHUNKS = 2
MESH = pl.DeviceIdType.MESH
F32 = jnp.float32
BF16 = jnp.bfloat16


def dot_nt(a, b):
    return lax.dot_general(a, b, (((1,), (1,)), ((), ())), preferred_element_type=F32)


def dot_nn(a, b):
    return lax.dot_general(a, b, (((1,), (0,)), ((), ())), preferred_element_type=F32)


def kernel(
    n_ep, ny, cap,
    tok_hbm, gain_hbm, ids_hbm, gates_hbm, wg_ref, wu_ref, wd_ref,
    out_ref,
    tok, gain, ids_v, gates,
    zsend, zrecv, xg, wland, wcat, wdn, gain_all, xs, part, chain, run, ssq, ssq_all,
    hid, po, xr, back, ret, tcol, mixed_v,
    z_ss, z_rs, r_ss, r_rs, w_ss, w_rs, g_ss, g_rs, x_ss, x_rs,
    y_ss, y_rs, q_ss, q_rs, h_ss, h_rs, o_ss, o_rs, l_sem, i_sem,
):
    nz = n_ep // 2
    rows = n_ep * PAD
    own = n_ep // ny
    oc = own // CHUNKS
    toks, feats = tok.shape
    experts = 2 * n_ep
    half = wg_ref.shape[1] // 2
    tiles = half // 128
    ep = lax.axis_index("ep")
    tp = lax.axis_index("tp")
    z, core = ep // 2, lax.rem(ep, 2)
    y, x = tp // NX, lax.rem(tp, NX)

    def z_peer(i):
        j, c = i // 2, lax.rem(i, 2)
        dz = nz // 2 + (1 - 2 * lax.rem(j, 2)) * ((j + 1) // 2)
        return 2 * lax.rem(z + dz, nz) + c

    def x_peer(k):
        return lax.rem(x + k, NX)

    def y_peer(k):
        return lax.rem(y + k, ny)

    def x_from(k):
        return lax.rem(x + NX - k, NX)

    def y_from(k):
        return lax.rem(y + ny - k, ny)

    def on_x(to):
        return dict(device_id=(ep, y * NX + to), device_id_type=MESH)

    def on_y(to):
        return dict(device_id=(ep, to * NX + x), device_id_type=MESH)

    def on_z(to):
        return dict(device_id=(to, tp), device_id_type=MESH)

    partner = z * 2 + (1 - core)
    x_steps = (2, 1, 3)
    y_steps = sorted(range(1, ny), key=lambda k: -min(k, ny - k))
    far = 2 * (nz - 1)

    barrier = pltpu.get_barrier_semaphore()

    def greet(i, carry):
        pl.semaphore_signal(barrier, inc=1, **on_z(z_peer(i)))
        return carry

    lax.fori_loop(0, far, greet, 0)
    pl.semaphore_signal(barrier, inc=1, **on_z(partner))
    for k in x_steps:
        pl.semaphore_signal(barrier, inc=1, **on_x(x_peer(k)))
    for k in y_steps:
        pl.semaphore_signal(barrier, inc=1, **on_y(y_peer(k)))

    loads = [
        pltpu.make_async_copy(a, b, i_sem.at[n])
        for n, (a, b) in enumerate(((ids_hbm, ids_v), (tok_hbm, tok), (gain_hbm, gain), (gates_hbm, gates)))
    ]
    for load in loads:
        load.start()

    def w_src(ref, to):
        return ref.at[to // 2, pl.ds(lax.rem(to, 2) * half, half), :]

    weights = (wg_ref, wu_ref, wd_ref)
    own_w = [pltpu.make_async_copy(w_src(ref, x), wland.at[n, x], l_sem.at[n]) for n, ref in enumerate(weights)]
    for copy in own_w:
        copy.start()
    ret[...] = jnp.zeros_like(ret)
    for load in loads:
        load.wait()

    ids = ids_v[...].astype(F32)
    e_iota = lax.broadcasted_iota(jnp.int32, (experts, toks), 0).astype(F32)
    m0, m1 = e_iota == ids[0:1, :], e_iota == ids[1:2, :]
    named = jnp.where(m0 | m1, 1.0, 0.0).astype(BF16)
    t_row = lax.broadcasted_iota(jnp.int32, (toks, toks), 0)
    t_col = lax.broadcasted_iota(jnp.int32, (toks, toks), 1)
    earlier = jnp.where(t_row < t_col, 1.0, 0.0).astype(BF16)
    before = dot_nn(named, earlier)
    target0 = ids[0:1, :] * PAD + jnp.sum(jnp.where(m0, before, 0.0), axis=0, keepdims=True)
    target1 = ids[1:2, :] * PAD + jnp.sum(jnp.where(m1, before, 0.0), axis=0, keepdims=True)
    chunk = min(256, experts * PAD)
    for n in range(experts * PAD // chunk):
        p_iota = (lax.broadcasted_iota(jnp.int32, (chunk, toks), 0) + n * chunk).astype(F32)
        pick = jnp.where((p_iota == target0) | (p_iota == target1), 1.0, 0.0).astype(BF16)
        block = dot_nn(pick, tok[...]).astype(BF16)
        zsend[pl.ds(n * chunk // PAD, chunk // PAD)] = block.reshape(chunk // PAD, PAD, feats)
    gain_all[x] = gain[...]

    pl.semaphore_wait(barrier, 2 * nz - 1 + (NX - 1) + (ny - 1))

    def z_copy(peer, slot):
        return pltpu.make_async_remote_copy(
            src_ref=zsend.at[pl.ds(2 * peer, 2), pl.ds(0, cap)], dst_ref=zrecv.at[:, slot, pl.ds(0, cap)],
            send_sem=z_ss, recv_sem=z_rs.at[slot], **on_z(peer),
        )

    def z_start(i, carry):
        z_copy(z_peer(i), ep).start()
        return carry

    lax.fori_loop(0, far, z_start, 0)
    z_copy(partner, ep).start()

    def w_copy(n, k, slot):
        return pltpu.make_async_remote_copy(
            src_ref=w_src(weights[n], x_peer(k)), dst_ref=wland.at[n, slot],
            send_sem=w_ss.at[n, k], recv_sem=w_rs.at[n, k], **on_x(x_peer(k)),
        )

    def g_copy(k, slot):
        return pltpu.make_async_remote_copy(
            src_ref=gain, dst_ref=gain_all.at[slot], send_sem=g_ss.at[k], recv_sem=g_rs.at[k], **on_x(x_peer(k))
        )

    for k in x_steps:
        g_copy(k, x).start()
    for n in range(2):
        for k in x_steps:
            w_copy(n, k, x).start()

    pad_rows = jnp.zeros((124, toks), F32)
    tcol[...] = jnp.concatenate([target0, target1, gates[...], pad_rows], axis=0).T

    def pass_on(src, s):
        for k in x_steps:
            pltpu.make_async_remote_copy(
                src_ref=src(x_peer(k) // 2), dst_ref=xg.at[x, s, pl.ds(0, cap)],
                send_sem=x_ss.at[k], recv_sem=x_rs.at[k], **on_x(x_peer(k)),
            ).start()

    def arrive(s):
        z_copy(s, s).wait_recv()
        pass_on(lambda e: zrecv.at[e, s, pl.ds(0, cap)], s)

    def z_arrive(i, carry):
        arrive(z_peer(far - 1 - i))
        return carry

    pass_on(lambda e: zsend.at[2 * ep + e, pl.ds(0, cap)], ep)
    arrive(partner)
    lax.fori_loop(0, far, z_arrive, 0)
    for k in x_steps:
        w_copy(2, k, x).start()
    xg[x] = zrecv[x // 2]
    xg[x, ep] = zsend[2 * ep + x // 2]

    for n in range(2):
        own_w[n].wait()
    for k in x_steps:
        g_copy(k, x_from(k)).wait_recv()
        for n in range(2):
            w_copy(n, k, x_from(k)).wait_recv()
    for s in range(NX):
        wcat[0:half, s * feats : (s + 1) * feats] = wland[0, s]
        wcat[half : 2 * half, s * feats : (s + 1) * feats] = wland[1, s]

    def x_all(k, slot):
        return pltpu.make_async_remote_copy(
            src_ref=zrecv.at[0, :, pl.ds(0, cap)], dst_ref=xg.at[slot, :, pl.ds(0, cap)],
            send_sem=x_ss.at[k], recv_sem=x_rs.at[k], **on_x(x_peer(k)),
        )

    for k in x_steps:
        x_all(k, x_from(k)).wait_recv()

    squares = jnp.zeros((rows, feats), F32)
    for s in range(NX):
        raw = xg[s].reshape(rows, feats).astype(F32)
        squares += raw * raw
        xs[:, :, s * feats : (s + 1) * feats] = (raw * gain_all[s]).astype(BF16).reshape(ny, own * PAD, feats)
    sums = jnp.sum(squares, axis=1, keepdims=True)
    lane = lax.broadcasted_iota(jnp.int32, (rows, 128), 1)
    row = lax.broadcasted_iota(jnp.int32, (rows, 128), 0)
    spread = jnp.where(lane == lax.rem(row, 128), sums, 0.0)
    groups = max(1, rows // 128)
    ssq[...] = jnp.concatenate(
        [jnp.sum(spread[g * 128 : (g + 1) * 128], axis=0, keepdims=True) for g in range(groups)], axis=0
    )

    def q_copy(k, slot):
        return pltpu.make_async_remote_copy(
            src_ref=ssq, dst_ref=ssq_all.at[slot], send_sem=q_ss.at[k], recv_sem=q_rs.at[k], **on_y(y_peer(k))
        )

    longest = ny // 2

    def length(c, way):
        return longest if (c + way) % 2 == 0 else ny - 1 - longest

    def target_of(c, way, s):
        ahead = length(c, way) - s + 1
        return y_peer(ahead) if way == 0 else y_from(ahead)

    def y_copy(c, way, s):
        to = y_peer(1) if way == 0 else y_from(1)
        if s == 1:
            src = part.at[target_of(c, way, s), pl.ds(c * oc, oc), :, pl.ds(0, cap)]
        else:
            src = run.at[way, c, s - 2, :, :, pl.ds(0, cap)]
        return pltpu.make_async_remote_copy(
            src_ref=src, dst_ref=chain.at[way, c, s - 1, :, :, pl.ds(0, cap)],
            send_sem=y_ss.at[way, c, s - 1], recv_sem=y_rs.at[way, c, s - 1], **on_y(to),
        )

    mc = ny * oc * PAD
    for c in range(CHUNKS):
        both = dot_nt(xs[:, c * oc * PAD : (c + 1) * oc * PAD, :].reshape(mc, NX * feats), wcat[...]).astype(BF16)
        for t in range(2 * tiles):
            part[:, c * oc : (c + 1) * oc, t] = both[:, t * 128 : (t + 1) * 128].reshape(ny, oc, PAD, 128)
        for way in range(2):
            if length(c, way):
                y_copy(c, way, 1).start()
    for k in y_steps:
        q_copy(k, y).start()
    ssq_all[y] = ssq[...]

    for s in range(2, longest + 1):
        for c in range(CHUNKS):
            for way in range(2):
                if length(c, way) >= s:
                    y_copy(c, way, s - 1).wait_recv()
                    mine = part[target_of(c, way, s), c * oc : (c + 1) * oc].astype(F32)
                    run[way, c, s - 2] = (chain[way, c, s - 2].astype(F32) + mine).astype(BF16)
                    y_copy(c, way, s).start()
        if s == 2:
            for k in y_steps:
                q_copy(k, y_from(k)).wait_recv()
            own_w[2].wait()
            for k in x_steps:
                w_copy(2, k, x_from(k)).wait_recv()
            for n in range(NX):
                wdn[:, n * feats : (n + 1) * feats] = wland[2, n]
    if longest < 2:
        for k in y_steps:
            q_copy(k, y_from(k)).wait_recv()
        own_w[2].wait()
        for k in x_steps:
            w_copy(2, k, x_from(k)).wait_recv()
        for n in range(NX):
            wdn[:, n * feats : (n + 1) * feats] = wland[2, n]

    stats = jnp.sum(ssq_all[...], axis=0)
    owned = own * PAD
    lane = lax.broadcasted_iota(jnp.int32, (owned, 128), 1)
    row = lax.broadcasted_iota(jnp.int32, (owned, 128), 0) + y * owned
    picked = jnp.zeros((owned, 128), F32)
    for g in range(groups):
        picked += jnp.where(row == lane + g * 128, stats[g : g + 1, :], 0.0)
    mean = jnp.sum(picked, axis=1, keepdims=True) / (feats * NX * ny)
    inverse = lax.rsqrt(mean + EPSILON)

    def h_copy(c, k, slot):
        return pltpu.make_async_remote_copy(
            src_ref=hid.at[slot, pl.ds(c * oc, oc), :, pl.ds(0, cap)],
            dst_ref=hid.at[slot, pl.ds(c * oc, oc), :, pl.ds(0, cap)],
            send_sem=h_ss.at[c, k], recv_sem=h_rs.at[c, k], **on_y(y_peer(k)),
        )

    for c in range(CHUNKS):
        ends = [(way, length(c, way)) for way in range(2) if length(c, way)]
        for way, s in ends:
            y_copy(c, way, s).wait_recv()
        inv = inverse[c * oc * PAD : (c + 1) * oc * PAD]

        def summed(t):
            total = part[y, c * oc : (c + 1) * oc, t].reshape(oc * PAD, 128).astype(F32)
            for way, s in ends:
                total += chain[way, c, s - 1, :, t].reshape(oc * PAD, 128).astype(F32)
            return total * inv

        for t in range(tiles):
            gate_act, up_act = summed(t), summed(tiles + t)
            hidden = (gate_act / (1.0 + jnp.exp(-gate_act)) * up_act).astype(BF16)
            hid[y, c * oc : (c + 1) * oc, t] = hidden.reshape(oc, PAD, 128)
        for k in y_steps:
            h_copy(c, k, y).start()

    def o_copy(c, k, slot):
        return pltpu.make_async_remote_copy(
            src_ref=po.at[x_peer(k), :, pl.ds(c * oc, oc), pl.ds(0, cap)],
            dst_ref=xr.at[slot, :, pl.ds(c * oc, oc), pl.ds(0, cap)],
            send_sem=o_ss.at[c, k], recv_sem=o_rs.at[c, k], **on_x(x_peer(k)),
        )

    for c in range(CHUNKS):
        for k in y_steps:
            h_copy(c, k, y_from(k)).wait_recv()
        held = jnp.concatenate(
            [hid[:, c * oc : (c + 1) * oc, t].reshape(mc, 128) for t in range(tiles)], axis=1
        )
        piece = dot_nn(held, wdn[...]).astype(BF16)
        for s in range(NX):
            po[s, :, c * oc : (c + 1) * oc] = piece[:, s * feats : (s + 1) * feats].reshape(ny, oc, PAD, feats)
        for k in x_steps:
            o_copy(c, k, x).start()
        xr[x, :, c * oc : (c + 1) * oc] = po[x, :, c * oc : (c + 1) * oc]

    def r_copy(s, slot):
        return pltpu.make_async_remote_copy(
            src_ref=back.at[:, s // own, lax.rem(s, own), pl.ds(0, cap)],
            dst_ref=ret.at[pl.ds(2 * slot, 2), pl.ds(0, cap)],
            send_sem=r_ss, recv_sem=r_rs, **on_z(s),
        )

    group = ep // own
    for c in range(CHUNKS):
        for k in x_steps:
            o_copy(c, k, x_from(k)).wait_recv()
        for e in range(2):
            a, b = (xr[2 * e + n, :, c * oc : (c + 1) * oc].astype(F32) for n in range(2))
            back[e, :, c * oc : (c + 1) * oc] = (a + b).astype(BF16)

        def r_start(i, carry):
            m, at = i // oc, lax.rem(i, oc)
            d = ny // 2 + (1 - 2 * lax.rem(m, 2)) * ((m + 1) // 2)
            s = own * lax.rem(group + d, ny) + c * oc + at

            @pl.when(s != ep)
            def _():
                r_copy(s, ep).start()

            return carry

        lax.fori_loop(0, ny * oc, r_start, 0)
    for e in range(2):
        ret[2 * ep + e, 0:cap] = back[e, group, lax.rem(ep, own), 0:cap]

    for k in x_steps:
        g_copy(k, x).wait_send()
        for n in range(3):
            w_copy(n, k, x).wait_send()
        x_all(k, x).wait_send()
    for k in y_steps:
        q_copy(k, y).wait_send()
        for c in range(CHUNKS):
            h_copy(c, k, y).wait_send()
    for c in range(CHUNKS):
        for way in range(2):
            for s in range(1, length(c, way) + 1):
                y_copy(c, way, s).wait_send()
        for k in x_steps:
            o_copy(c, k, x).wait_send()
    everyone = pl.ds(0, 2 * (n_ep - 1))
    pltpu.make_async_copy(
        zsend.at[everyone, pl.ds(0, cap)], zsend.at[everyone, pl.ds(0, cap)], z_ss
    ).wait()

    pltpu.make_async_copy(ret.at[everyone, pl.ds(0, cap)], ret.at[everyone, pl.ds(0, cap)], r_rs).wait()
    answers = ret[...].reshape(experts * PAD, feats)
    p_iota = lax.broadcasted_iota(jnp.int32, (toks, experts * PAD), 1).astype(F32)
    mixed = jnp.zeros((toks, feats), F32)
    for k in range(2):
        pick = jnp.where(p_iota == tcol[:, k : k + 1], 1.0, 0.0).astype(BF16)
        mixed += dot_nn(pick, answers) * tcol[:, 2 + k : 3 + k]
    mixed_v[...] = mixed.astype(BF16)
    write = pltpu.make_async_copy(mixed_v, out_ref, i_sem.at[0])
    write.start()
    pltpu.make_async_copy(ret.at[everyone, pl.ds(0, cap)], ret.at[everyone, pl.ds(0, cap)], r_ss).wait()
    write.wait()


def layer(n_ep, n_tp, tokens, norm_gain, route_ids, route_gates, w_gate, w_up, w_down):
    toks, feats = tokens.shape
    ny = n_tp // NX
    experts = 2 * n_ep
    cap = max(2, (5 * toks * 2 + 4 * experts - 1) // (4 * experts))
    half = w_gate.shape[1] // 2
    tiles = half // 128
    own = n_ep // ny
    oc = own // CHUNKS
    rows = n_ep * PAD
    groups = max(1, rows // 128)
    hops = ny // 2
    dma = pltpu.SemaphoreType.DMA
    hbm = pl.BlockSpec(memory_space=pl.ANY)
    return pl.pallas_call(
        functools.partial(kernel, n_ep, ny, cap),
        out_shape=jax.ShapeDtypeStruct((toks, feats), BF16),
        in_specs=[hbm] * 7,
        out_specs=hbm,
        scratch_shapes=[
            pltpu.VMEM((toks, feats), BF16),
            pltpu.VMEM((1, feats), F32),
            pltpu.VMEM((2, toks), jnp.int32),
            pltpu.VMEM((2, toks), F32),
            pltpu.VMEM((experts, PAD, feats), BF16),
            pltpu.VMEM((2, n_ep, PAD, feats), BF16),
            pltpu.VMEM((NX, n_ep, PAD, feats), BF16),
            pltpu.VMEM((3, NX, half, feats), BF16),
            pltpu.VMEM((2 * half, NX * feats), BF16),
            pltpu.VMEM((half, NX * feats), BF16),
            pltpu.VMEM((NX, 1, feats), F32),
            pltpu.VMEM((ny, own * PAD, NX * feats), BF16),
            pltpu.VMEM((ny, own, 2 * tiles, PAD, 128), BF16),
            pltpu.VMEM((2, CHUNKS, hops, oc, 2 * tiles, PAD, 128), BF16),
            pltpu.VMEM((2, CHUNKS, max(1, hops - 1), oc, 2 * tiles, PAD, 128), BF16),
            pltpu.VMEM((groups, 128), F32),
            pltpu.VMEM((ny, groups, 128), F32),
            pltpu.VMEM((ny, own, tiles, PAD, 128), BF16),
            pltpu.VMEM((NX, ny, own, PAD, feats), BF16),
            pltpu.VMEM((NX, ny, own, PAD, feats), BF16),
            pltpu.VMEM((2, ny, own, PAD, feats), BF16),
            pltpu.VMEM((experts, PAD, feats), BF16),
            pltpu.VMEM((toks, 128), F32),
            pltpu.VMEM((toks, feats), BF16),
            dma, dma((n_ep,)), dma, dma,
            dma((3, NX)), dma((3, NX)), dma((NX,)), dma((NX,)), dma((NX,)), dma((NX,)),
            dma((2, CHUNKS, hops)), dma((2, CHUNKS, hops)), dma((ny,)), dma((ny,)),
            dma((CHUNKS, ny)), dma((CHUNKS, ny)), dma((CHUNKS, NX)), dma((CHUNKS, NX)), dma((3,)), dma((4,)),
        ],
        compiler_params=pltpu.CompilerParams(collective_id=0, has_side_effects=True),
        name="routed_layer",
    )(tokens, norm_gain.reshape(1, feats), route_ids.T, route_gates.T, w_gate, w_up, w_down)


def solution(mesh):
    placed = (
        P("ep", "tp"),
        P("tp"),
        P("ep", None),
        P("ep", None),
        P("ep", None, "tp"),
        P("ep", None, "tp"),
        P("ep", None, "tp"),
    )
    body = functools.partial(layer, mesh.shape["ep"], mesh.shape["tp"])
    return jax.shard_map(body, mesh=mesh, in_specs=placed, out_specs=P("ep", "tp"), check_vma=False)
```

time: 86.5 us -> 75.8 us (0.88)
  Pallas kernels: 84.8 us -> 73.9 us
    pallas_call x1, Pallas kernels: 84.8 us -> 73.9 us  [layer(): pl.pallas_call(functools.partial(kernel, n_ep, ny, cap), out_shape=jax.Sh...]
where the time goes in v2:
time: 75.8 us; the launch traced here: 75.4 us
  Pallas kernels  73.9 us (97%)
  local copies, waits for them, and re-layouts  1.47 us (2%)
    pallas_call x1, Pallas kernels, layer(): pl.pallas_call(functools.partial(kernel, n_ep, ny, cap), out_shape=jax.Sh...  73.9 us

profile of v2, /device:TPU:1, one launch (start us, length us, event | category | flops | bytes accessed | tf_op | source)
XLA Modules:
  0.0 75.4 jit_solution(8594342186351912090)
XLA Ops:
  0.0 73.9 %routed_layer.1 = bf16[256,128]{1,0:T(8,128)(2,1)} custom-call(bf16[256,128]{1,0:T(8,128)(2,1)} %tok_hbm.1, f32[1,128]{1,0:T(1,128)} %bitcast.5, s32[2,256]{1,0:T(2,128)} %bitcast.3, f32[2,256]{1,0:T(2,128)} %bitcast.4, bf16[2,768,128]{2,1,0:T(8,128)(2,1)} %wg_ref.1, bf16[2,768,128]{2,1,0:T(8,128)(2,1)} %wu_ref.1, bf16[2,768,128]{2,1,0:T(8,128)(2,1)} %wd_ref.1), custom_call_target="tpu_custom_call" | custom-call | tf_op jit(solution)/shard_map/routed_layer/pallas_call | solution.py:417
  73.9 1.5 %copy.9 = bf16[256,128]{1,0:T(8,128)(2,1)} copy(bf16[256,128]{1,0:T(8,128)(2,1)} %routed_layer.1) | data formatting | bytes 131072

commit v3 on v0

v3 whole, which is shorter than its diff:
```python
import functools

import jax
import jax.numpy as jnp
from jax import lax
from jax.experimental import pallas as pl
from jax.experimental.pallas import tpu as pltpu
from jax.sharding import PartitionSpec as P

EPSILON = 1e-06
NX = 4
PAD = 16
MESH = pl.DeviceIdType.MESH
F32 = jnp.float32
BF16 = jnp.bfloat16


def dot_nt(a, b):
    return lax.dot_general(a, b, (((1,), (1,)), ((), ())), preferred_element_type=F32)


def dot_nn(a, b):
    return lax.dot_general(a, b, (((1,), (0,)), ((), ())), preferred_element_type=F32)


def kernel(
    n_ep, ny, cap,
    tok_hbm, gain_hbm, ids_hbm, gates_hbm, wg_ref, wu_ref, wd_ref,
    out_ref,
    tok, gain, ids_v, gates,
    zsend, zrecv, xg, wland, wcat, wdn, gain_all, xs, part, direct, ssq, ssq_all,
    hid, po, xr, back, ret, tcol, picks,
    z_ss, z_rs, r_ss, r_rs, w_ss, w_rs, g_ss, g_rs, x_ss, x_rs,
    d_ss, d_rs, q_ss, q_rs, h_ss, h_rs, o_ss, o_rs, l_sem, i_sem,
):
    nz = n_ep // 2
    chunks = n_ep // ny
    rows = ny * PAD
    toks, feats = tok.shape
    experts = 2 * n_ep
    half = wg_ref.shape[1] // 2
    tiles = half // 128
    ep = lax.axis_index("ep")
    tp = lax.axis_index("tp")
    z, core = ep // 2, lax.rem(ep, 2)
    y, x = tp // NX, lax.rem(tp, NX)
    filled = pl.ds(0, cap)

    def z_peer(i):
        j, c = i // 2, lax.rem(i, 2)
        dz = nz // 2 + (1 - 2 * lax.rem(j, 2)) * ((j + 1) // 2)
        return 2 * lax.rem(z + dz, nz) + c

    def x_peer(k):
        return lax.rem(x + k, NX)

    def y_peer(k):
        return lax.rem(y + k, ny)

    def on_x(k):
        return dict(device_id=(ep, y * NX + x_peer(k)), device_id_type=MESH)

    def on_y(k):
        return dict(device_id=(ep, y_peer(k) * NX + x), device_id_type=MESH)

    def on_z(to):
        return dict(device_id=(to, tp), device_id_type=MESH)

    def settle(ref, sem):
        pltpu.make_async_copy(ref, ref, sem).wait()

    partner = z * 2 + (1 - core)
    x_steps = (2, 1, 3)
    y_steps = sorted(range(1, ny), key=lambda k: -min(k, ny - k))
    far = 2 * (nz - 1)

    barrier = pltpu.get_barrier_semaphore()

    def greet(i, carry):
        pl.semaphore_signal(barrier, inc=1, **on_z(z_peer(i)))
        return carry

    lax.fori_loop(0, far, greet, 0)
    pl.semaphore_signal(barrier, inc=1, **on_z(partner))
    for k in x_steps:
        pl.semaphore_signal(barrier, inc=1, **on_x(k))
    for k in y_steps:
        pl.semaphore_signal(barrier, inc=1, **on_y(k))

    loads = [
        pltpu.make_async_copy(a, b, i_sem.at[n])
        for n, (a, b) in enumerate(((ids_hbm, ids_v), (tok_hbm, tok), (gain_hbm, gain), (gates_hbm, gates)))
    ]
    for load in loads:
        load.start()

    def w_src(ref, to):
        return ref.at[to // 2, pl.ds(lax.rem(to, 2) * half, half), :]

    weights = (wg_ref, wu_ref, wd_ref)
    for n, ref in enumerate(weights):
        pltpu.make_async_copy(w_src(ref, x), wland.at[n, x], l_sem).start()
    ret[...] = jnp.zeros_like(ret)
    for load in loads:
        load.wait()

    ids = ids_v[...].astype(F32)
    e_iota = lax.broadcasted_iota(jnp.int32, (experts, toks), 0).astype(F32)
    m0, m1 = e_iota == ids[0:1, :], e_iota == ids[1:2, :]
    named = jnp.where(m0 | m1, 1.0, 0.0).astype(BF16)
    t_row = lax.broadcasted_iota(jnp.int32, (toks, toks), 0)
    t_col = lax.broadcasted_iota(jnp.int32, (toks, toks), 1)
    earlier = jnp.where(t_row < t_col, 1.0, 0.0).astype(BF16)
    before = dot_nn(named, earlier)
    target0 = ids[0:1, :] * PAD + jnp.sum(jnp.where(m0, before, 0.0), axis=0, keepdims=True)
    target1 = ids[1:2, :] * PAD + jnp.sum(jnp.where(m1, before, 0.0), axis=0, keepdims=True)
    size = min(256, experts * PAD)
    for n in range(experts * PAD // size):
        p_iota = (lax.broadcasted_iota(jnp.int32, (size, toks), 0) + n * size).astype(F32)
        pick = jnp.where((p_iota == target0) | (p_iota == target1), 1.0, 0.0).astype(BF16)
        block = dot_nn(pick, tok[...]).astype(BF16)
        zsend[pl.ds(n * size // PAD, size // PAD)] = block.reshape(size // PAD, PAD, feats)
    gain_all[x] = gain[...]

    pl.semaphore_wait(barrier, 2 * nz - 1 + (NX - 1) + (ny - 1))

    def z_copy(peer):
        return pltpu.make_async_remote_copy(
            src_ref=zsend.at[pl.ds(2 * peer, 2), filled], dst_ref=zrecv.at[:, ep, filled],
            send_sem=z_ss, recv_sem=z_rs.at[ep // ny], **on_z(peer),
        )

    def z_start(i, carry):
        z_copy(z_peer(i)).start()
        return carry

    lax.fori_loop(0, far, z_start, 0)
    z_copy(partner).start()

    def send_weight(n):
        for k in x_steps:
            pltpu.make_async_remote_copy(
                src_ref=w_src(weights[n], x_peer(k)), dst_ref=wland.at[n, x],
                send_sem=w_ss, recv_sem=w_rs.at[n], **on_x(k),
            ).start()

    for k in x_steps:
        pltpu.make_async_remote_copy(
            src_ref=gain, dst_ref=gain_all.at[x], send_sem=g_ss, recv_sem=g_rs, **on_x(k)
        ).start()
    send_weight(0)
    send_weight(1)
    for e in range(2):
        zrecv[e, ep] = zsend[2 * ep + e]

    pad_rows = jnp.zeros((124, toks), F32)
    tcol[...] = jnp.concatenate([target0, target1, gates[...], pad_rows], axis=0).T

    def arrive(c):
        @pl.when(ep // ny == c)
        def _():
            settle(zrecv.at[:, pl.ds(0, ny - 1), filled], z_rs.at[c])

        @pl.when(ep // ny != c)
        def _():
            settle(zrecv.at[:, pl.ds(0, ny), filled], z_rs.at[c])

        for k in x_steps:
            pltpu.make_async_remote_copy(
                src_ref=zrecv.at[x_peer(k) // 2, pl.ds(c * ny, ny), filled],
                dst_ref=xg.at[x, pl.ds(c * ny, ny), filled],
                send_sem=x_ss, recv_sem=x_rs.at[c], **on_x(k),
            ).start()
        xg[x, c * ny : (c + 1) * ny] = zrecv[x // 2, c * ny : (c + 1) * ny]

    lane = lax.broadcasted_iota(jnp.int32, (rows, 128), 1)
    row = lax.broadcasted_iota(jnp.int32, (rows, 128), 0)

    def gate_up(c):
        settle(xg.at[pl.ds(0, NX - 1), pl.ds(0, ny), filled], x_rs.at[c])
        squares = jnp.zeros((rows, feats), F32)
        for s in range(NX):
            raw = xg[s, c * ny : (c + 1) * ny].reshape(rows, feats).astype(F32)
            squares += raw * raw
            xs[:, s * feats : (s + 1) * feats] = (raw * gain_all[s]).astype(BF16)
        both = dot_nt(xs[...], wcat[...]).astype(BF16)
        for t in range(2 * tiles):
            part[c, :, t] = both[:, t * 128 : (t + 1) * 128].reshape(ny, PAD, 128)
        for k in y_steps:
            pltpu.make_async_remote_copy(
                src_ref=part.at[c, y_peer(k), :, filled], dst_ref=direct.at[c, k - 1, :, filled],
                send_sem=d_ss, recv_sem=d_rs.at[c], **on_y(k),
            ).start()
        sums = jnp.sum(squares, axis=1, keepdims=True)
        ssq[c] = jnp.sum(jnp.where(lane == row, sums, 0.0), axis=0, keepdims=True)
        for k in y_steps:
            pltpu.make_async_remote_copy(
                src_ref=ssq.at[c], dst_ref=ssq_all.at[c, k - 1], send_sem=q_ss, recv_sem=q_rs.at[c], **on_y(k)
            ).start()

    def activate(c):
        settle(ssq_all.at[c, pl.ds(0, ny - 1)], q_rs.at[c])
        stats = ssq[c] + jnp.sum(ssq_all[c], axis=0)
        held = jnp.where(row[:PAD] + y * PAD == lane[:PAD], stats, 0.0)
        mean = jnp.sum(held, axis=1, keepdims=True) / (feats * NX * ny)
        inverse = lax.rsqrt(mean + EPSILON)
        settle(direct.at[c, pl.ds(0, ny - 1), :, filled], d_rs.at[c])

        def summed(t):
            total = part[c, y, t].astype(F32)
            for k in range(ny - 1):
                total += direct[c, k, t].astype(F32)
            return total * inverse

        for t in range(tiles):
            gate_act, up_act = summed(t), summed(tiles + t)
            hid[c, y, t] = (gate_act / (1.0 + jnp.exp(-gate_act)) * up_act).astype(BF16)
        for k in y_steps:
            pltpu.make_async_remote_copy(
                src_ref=hid.at[c, y, :, filled], dst_ref=hid.at[c, y, :, filled],
                send_sem=h_ss, recv_sem=h_rs.at[c], **on_y(k),
            ).start()

    def down(c):
        settle(hid.at[c, pl.ds(0, ny - 1), :, filled], h_rs.at[c])
        held = jnp.concatenate([hid[c, :, t].reshape(rows, 128) for t in range(tiles)], axis=1)
        piece = dot_nn(held, wdn[...]).astype(BF16)
        for s in range(NX):
            po[s, c] = piece[:, s * feats : (s + 1) * feats].reshape(ny, PAD, feats)
        for k in x_steps:
            pltpu.make_async_remote_copy(
                src_ref=po.at[x_peer(k), c, :, filled], dst_ref=xr.at[x, c, :, filled],
                send_sem=o_ss, recv_sem=o_rs.at[c], **on_x(k),
            ).start()
        xr[x, c] = po[x, c]

    def r_copy(s):
        return pltpu.make_async_remote_copy(
            src_ref=back.at[:, s, filled], dst_ref=ret.at[pl.ds(2 * ep, 2), filled],
            send_sem=r_ss, recv_sem=r_rs, **on_z(s),
        )

    def give_back(c):
        settle(xr.at[pl.ds(0, NX - 1), 0, :, filled], o_rs.at[c])
        for e in range(2):
            back[e, c * ny : (c + 1) * ny] = (xr[2 * e, c].astype(F32) + xr[2 * e + 1, c].astype(F32)).astype(BF16)

        def r_start(i, carry):
            @pl.when(c * ny + i != ep)
            def _():
                r_copy(c * ny + i).start()

            return carry

        lax.fori_loop(0, ny, r_start, 0)

    def join_gate_up():
        settle(wland.at[:, 0], l_sem)
        settle(gain_all.at[pl.ds(0, NX - 1)], g_rs)
        for n in range(2):
            settle(wland.at[n, pl.ds(0, NX - 1)], w_rs.at[n])
            for s in range(NX):
                wcat[n * half : (n + 1) * half, s * feats : (s + 1) * feats] = wland[n, s]

    def join_down():
        settle(wland.at[2, pl.ds(0, NX - 1)], w_rs.at[2])
        for s in range(NX):
            wdn[:, s * feats : (s + 1) * feats] = wland[2, s]

    ahead = min(2, chunks)
    for c in range(ahead):
        arrive(c)
    join_gate_up()
    for c in range(ahead):
        gate_up(c)
        if c + ahead < chunks:
            arrive(c + ahead)
    send_weight(2)
    p_iota = lax.broadcasted_iota(jnp.int32, (toks, experts * PAD), 1).astype(F32)
    for k in range(2):
        picks[k] = jnp.where(p_iota == tcol[:, k : k + 1], 1.0, 0.0).astype(BF16)
    for c in range(ahead):
        activate(c)
        if c + ahead < chunks:
            gate_up(c + ahead)
    join_down()
    down(0)
    for c in range(chunks):
        if c + ahead < chunks:
            activate(c + ahead)
        if c + 1 < chunks:
            down(c + 1)
        give_back(c)
    for e in range(2):
        ret[2 * ep + e, 0:cap] = back[e, ep, 0:cap]

    settle(zsend.at[pl.ds(0, 2 * (n_ep - 1)), filled], z_ss)
    settle(gain_all.at[pl.ds(0, NX - 1)], g_ss)
    settle(wland.at[:, pl.ds(0, NX - 1)], w_ss)
    settle(xg.at[pl.ds(0, NX - 1), :, filled], x_ss)
    settle(direct.at[:, :, :, filled], d_ss)
    settle(ssq_all, q_ss)
    settle(hid.at[:, pl.ds(0, ny - 1), :, filled], h_ss)
    settle(xr.at[pl.ds(0, NX - 1), :, :, filled], o_ss)

    everyone = ret.at[pl.ds(0, 2 * (n_ep - 1)), filled]
    settle(everyone, r_rs)
    answers = ret[...].reshape(experts * PAD, feats)
    out_ref[...] = (dot_nn(picks[0], answers) * tcol[:, 2:3] + dot_nn(picks[1], answers) * tcol[:, 3:4]).astype(BF16)
    settle(everyone, r_ss)


def layer(n_ep, n_tp, tokens, norm_gain, route_ids, route_gates, w_gate, w_up, w_down):
    toks, feats = tokens.shape
    ny = n_tp // NX
    chunks = n_ep // ny
    experts = 2 * n_ep
    cap = max(2, (5 * toks * 2 + 4 * experts - 1) // (4 * experts))
    half = w_gate.shape[1] // 2
    tiles = half // 128
    dma = pltpu.SemaphoreType.DMA
    each = pltpu.SemaphoreType.DMA((chunks,))
    hbm = pl.BlockSpec(memory_space=pl.ANY)
    mixed = pl.pallas_call(
        functools.partial(kernel, n_ep, ny, cap),
        out_shape=pltpu.VMEM((toks, feats), BF16),
        in_specs=[hbm] * 7,
        out_specs=pl.BlockSpec(memory_space=pltpu.VMEM),
        scratch_shapes=[
            pltpu.VMEM((toks, feats), BF16),
            pltpu.VMEM((1, feats), F32),
            pltpu.VMEM((2, toks), jnp.int32),
            pltpu.VMEM((2, toks), F32),
            pltpu.VMEM((experts, PAD, feats), BF16),
            pltpu.VMEM((2, n_ep, PAD, feats), BF16),
            pltpu.VMEM((NX, n_ep, PAD, feats), BF16),
            pltpu.VMEM((3, NX, half, feats), BF16),
            pltpu.VMEM((2 * half, NX * feats), BF16),
            pltpu.VMEM((half, NX * feats), BF16),
            pltpu.VMEM((NX, 1, feats), F32),
            pltpu.VMEM((ny * PAD, NX * feats), BF16),
            pltpu.VMEM((chunks, ny, 2 * tiles, PAD, 128), BF16),
            pltpu.VMEM((chunks, ny - 1, 2 * tiles, PAD, 128), BF16),
            pltpu.VMEM((chunks, 1, 128), F32),
            pltpu.VMEM((chunks, ny - 1, 1, 128), F32),
            pltpu.VMEM((chunks, ny, tiles, PAD, 128), BF16),
            pltpu.VMEM((NX, chunks, ny, PAD, feats), BF16),
            pltpu.VMEM((NX, chunks, ny, PAD, feats), BF16),
            pltpu.VMEM((2, n_ep, PAD, feats), BF16),
            pltpu.VMEM((experts, PAD, feats), BF16),
            pltpu.VMEM((toks, 128), F32),
            pltpu.VMEM((2, toks, experts * PAD), BF16),
            dma, each, dma, dma, dma, dma((3,)), dma, dma, dma, each,
            dma, each, dma, each, dma, each, dma, each, dma, dma((4,)),
        ],
        compiler_params=pltpu.CompilerParams(collective_id=0, has_side_effects=True),
        name="routed_layer",
    )(tokens, norm_gain.reshape(1, feats), route_ids.T, route_gates.T, w_gate, w_up, w_down)
    return mixed


def solution(mesh):
    placed = (
        P("ep", "tp"),
        P("tp"),
        P("ep", None),
        P("ep", None),
        P("ep", None, "tp"),
        P("ep", None, "tp"),
        P("ep", None, "tp"),
    )
    body = functools.partial(layer, mesh.shape["ep"], mesh.shape["tp"])
    return jax.shard_map(body, mesh=mesh, in_specs=placed, out_specs=P("ep", "tp"), check_vma=False)
```

time: 177 us -> 64.4 us (0.36)
  the two profiles are of different devices: /device:TPU:1 before, /device:TPU:8 now
where the time goes in v3:
time: 64.4 us; the launch traced here: 64.2 us
  Pallas kernels  63.5 us (99%)
    pallas_call x1, Pallas kernels, layer(): pl.pallas_call(functools.partial(kernel, n_ep, ny, cap), out_shape=pltpu....  63.5 us

profile of v3, /device:TPU:8, one launch (start us, length us, event | category | flops | bytes accessed | tf_op | source)
XLA Modules:
  0.0 64.2 jit_solution(4402745377217653528)
XLA Ops:
  0.0 63.5 %routed_layer.1 = bf16[256,128]{1,0:T(8,128)(2,1)S(1)} custom-call(bf16[256,128]{1,0:T(8,128)(2,1)} %tok_hbm.1, f32[1,128]{1,0:T(1,128)} %bitcast.5, s32[2,256]{1,0:T(2,128)} %bitcast.3, f32[2,256]{1,0:T(2,128)} %bitcast.4, bf16[2,768,128]{2,1,0:T(8,128)(2,1)} %wg_ref.1, bf16[2,768,128]{2,1,0:T(8,128)(2,1)} %wu_ref.1, bf16[2,768,128]{2,1,0:T(8,128)(2,1)} %wd_ref.1), custom_call_target="tpu_custom_call" | custom-call | tf_op jit(solution)/shard_map/routed_layer/pallas_call | solution.py:324
  63.6 0.6 copy.9

commit v4 on v3

--- a/solution.py
+++ b/solution.py
@@ -29,9 +29,9 @@
     out_ref,
     tok, gain, ids_v, gates,
     zsend, zrecv, xg, wland, wcat, wdn, gain_all, xs, part, direct, ssq, ssq_all,
-    hid, po, xr, back, ret, tcol, picks,
+    hid, po, xr, back, ret, tcol, picks, staged, chain, run,
     z_ss, z_rs, r_ss, r_rs, w_ss, w_rs, g_ss, g_rs, x_ss, x_rs,
-    d_ss, d_rs, q_ss, q_rs, h_ss, h_rs, o_ss, o_rs, l_sem, i_sem,
+    d_ss, d_rs, q_ss, q_rs, h_ss, h_rs, o_ss, o_rs, l_sem, i_sem, y_ss, y_rs,
 ):
     nz = n_ep // 2
     chunks = n_ep // ny
@@ -51,6 +51,18 @@
         dz = nz // 2 + (1 - 2 * lax.rem(j, 2)) * ((j + 1) // 2)
         return 2 * lax.rem(z + dz, nz) + c
 
+    side = nz // 2
+
+    def slot_of(s):
+        lo = lax.rem(s // 2, side)
+        return 2 * (4 * (lo // 2) + 2 * (s // 2 // side) + lax.rem(lo, 2)) + lax.rem(s, 2)
+
+    def source_of(n):
+        v = n // 2
+        return 2 * (side * lax.rem(v // 2, 2) + 2 * (v // 4) + lax.rem(v, 2)) + lax.rem(n, 2)
+
+    mine = slot_of(ep)
+
     def x_peer(k):
         return lax.rem(x + k, NX)
 
@@ -73,6 +85,13 @@
     x_steps = (2, 1, 3)
     y_steps = sorted(range(1, ny), key=lambda k: -min(k, ny - k))
     far = 2 * (nz - 1)
+
+    loads = [
+        pltpu.make_async_copy(a, b, i_sem.at[n])
+        for n, (a, b) in enumerate(((ids_hbm, ids_v), (tok_hbm, tok), (gain_hbm, gain), (gates_hbm, gates)))
+    ]
+    for load in loads[:2]:
+        load.start()
 
     barrier = pltpu.get_barrier_semaphore()
 
@@ -87,19 +106,15 @@
     for k in y_steps:
         pl.semaphore_signal(barrier, inc=1, **on_y(k))
 
-    loads = [
-        pltpu.make_async_copy(a, b, i_sem.at[n])
-        for n, (a, b) in enumerate(((ids_hbm, ids_v), (tok_hbm, tok), (gain_hbm, gain), (gates_hbm, gates)))
-    ]
-    for load in loads:
+    for load in loads[2:]:
         load.start()
 
-    def w_src(ref, to):
-        return ref.at[to // 2, pl.ds(lax.rem(to, 2) * half, half), :]
+    def w_src(n, to):
+        return staged.at[n, to // 2, pl.ds(pl.multiple_of(lax.rem(to, 2) * half, half), half)]
 
     weights = (wg_ref, wu_ref, wd_ref)
     for n, ref in enumerate(weights):
-        pltpu.make_async_copy(w_src(ref, x), wland.at[n, x], l_sem).start()
+        pltpu.make_async_copy(ref, staged.at[n], l_sem).start()
     ret[...] = jnp.zeros_like(ret)
     for load in loads:
         load.wait()
@@ -121,26 +136,24 @@
         block = dot_nn(pick, tok[...]).astype(BF16)
         zsend[pl.ds(n * size // PAD, size // PAD)] = block.reshape(size // PAD, PAD, feats)
     gain_all[x] = gain[...]
-
     pl.semaphore_wait(barrier, 2 * nz - 1 + (NX - 1) + (ny - 1))
+    settle(staged, l_sem)
 
     def z_copy(peer):
         return pltpu.make_async_remote_copy(
-            src_ref=zsend.at[pl.ds(2 * peer, 2), filled], dst_ref=zrecv.at[:, ep, filled],
-            send_sem=z_ss, recv_sem=z_rs.at[ep // ny], **on_z(peer),
+            src_ref=zsend.at[pl.ds(2 * peer, 2), filled], dst_ref=zrecv.at[:, mine, filled],
+            send_sem=z_ss, recv_sem=z_rs.at[mine // ny], **on_z(peer),
         )
 
     def z_start(i, carry):
         z_copy(z_peer(i)).start()
         return carry
 
-    lax.fori_loop(0, far, z_start, 0)
-    z_copy(partner).start()
 
     def send_weight(n):
         for k in x_steps:
             pltpu.make_async_remote_copy(
-                src_ref=w_src(weights[n], x_peer(k)), dst_ref=wland.at[n, x],
+                src_ref=w_src(n, x_peer(k)), dst_ref=wland.at[n, x],
                 send_sem=w_ss, recv_sem=w_rs.at[n], **on_x(k),
             ).start()
 
@@ -150,18 +163,22 @@
         ).start()
     send_weight(0)
     send_weight(1)
+    lax.fori_loop(0, far, z_start, 0)
+    z_copy(partner).start()
     for e in range(2):
-        zrecv[e, ep] = zsend[2 * ep + e]
+        zrecv[e, mine] = zsend[2 * ep + e]
+    for n in range(3):
+        wland[n, x] = w_src(n, x)[...]
 
     pad_rows = jnp.zeros((124, toks), F32)
     tcol[...] = jnp.concatenate([target0, target1, gates[...], pad_rows], axis=0).T
 
     def arrive(c):
-        @pl.when(ep // ny == c)
+        @pl.when(mine // ny == c)
         def _():
             settle(zrecv.at[:, pl.ds(0, ny - 1), filled], z_rs.at[c])
 
-        @pl.when(ep // ny != c)
+        @pl.when(mine // ny != c)
         def _():
             settle(zrecv.at[:, pl.ds(0, ny), filled], z_rs.at[c])
 
@@ -172,6 +189,40 @@
                 send_sem=x_ss, recv_sem=x_rs.at[c], **on_x(k),
             ).start()
         xg[x, c * ny : (c + 1) * ny] = zrecv[x // 2, c * ny : (c + 1) * ny]
+
+    longest = ny // 2
+    straight = chunks // 2
+
+    def length(c, way):
+        return longest if (c + way) % 2 == 0 else ny - 1 - longest
+
+    def place(c, way, s):
+        return s - 1 + (length(c, 0) if way else 0)
+
+    def towards(c, way, s):
+        left = length(c, way) - s + 1
+        return y_peer(left if way == 0 else ny - left)
+
+    def chain_start(c, way, s):
+        n, at = c - straight, place(c, way, s)
+        src = part.at[c, towards(c, way, s)] if s == 1 else run.at[n, at]
+        pltpu.make_async_remote_copy(
+            src_ref=src.at[:, filled], dst_ref=chain.at[n, at, :, filled],
+            send_sem=y_ss, recv_sem=y_rs.at[n, at], **on_y(1 if way == 0 else ny - 1),
+        ).start()
+
+    def chain_end(c, way, s):
+        n, at = c - straight, place(c, way, s)
+        settle(chain.at[n, at, :, filled], y_rs.at[n, at])
+        return chain.at[n, at]
+
+    def hop(s):
+        for c in range(straight, chunks):
+            for way in range(2):
+                if length(c, way) >= s:
+                    came = chain_end(c, way, s - 1)[...].astype(F32)
+                    run[c - straight, place(c, way, s)] = (came + part[c, towards(c, way, s)].astype(F32)).astype(BF16)
+                    chain_start(c, way, s)
 
     lane = lax.broadcasted_iota(jnp.int32, (rows, 128), 1)
     row = lax.broadcasted_iota(jnp.int32, (rows, 128), 0)
@@ -186,30 +237,45 @@
         both = dot_nt(xs[...], wcat[...]).astype(BF16)
         for t in range(2 * tiles):
             part[c, :, t] = both[:, t * 128 : (t + 1) * 128].reshape(ny, PAD, 128)
+        sums = jnp.sum(squares, axis=1, keepdims=True)
+        ssq[c] = jnp.sum(jnp.where(lane == row, sums, 0.0), axis=0, keepdims=True)
+
+    def send_stats(c):
+        for k in y_steps:
+            pltpu.make_async_remote_copy(
+                src_ref=ssq.at[c], dst_ref=ssq_all.at[c, k - 1], send_sem=q_ss, recv_sem=q_rs.at[c], **on_y(k)
+            ).start()
+
+    def send_sums(c):
         for k in y_steps:
             pltpu.make_async_remote_copy(
                 src_ref=part.at[c, y_peer(k), :, filled], dst_ref=direct.at[c, k - 1, :, filled],
                 send_sem=d_ss, recv_sem=d_rs.at[c], **on_y(k),
             ).start()
-        sums = jnp.sum(squares, axis=1, keepdims=True)
-        ssq[c] = jnp.sum(jnp.where(lane == row, sums, 0.0), axis=0, keepdims=True)
-        for k in y_steps:
-            pltpu.make_async_remote_copy(
-                src_ref=ssq.at[c], dst_ref=ssq_all.at[c, k - 1], send_sem=q_ss, recv_sem=q_rs.at[c], **on_y(k)
-            ).start()
-
-    def activate(c):
+        send_stats(c)
+
+    def send_chain(c):
+        for way in range(2):
+            if length(c, way):
+                chain_start(c, way, 1)
+        send_stats(c)
+
+    def activate(c, chained=False):
         settle(ssq_all.at[c, pl.ds(0, ny - 1)], q_rs.at[c])
         stats = ssq[c] + jnp.sum(ssq_all[c], axis=0)
         held = jnp.where(row[:PAD] + y * PAD == lane[:PAD], stats, 0.0)
         mean = jnp.sum(held, axis=1, keepdims=True) / (feats * NX * ny)
         inverse = lax.rsqrt(mean + EPSILON)
-        settle(direct.at[c, pl.ds(0, ny - 1), :, filled], d_rs.at[c])
+        if chained:
+            terms = [chain_end(c, way, length(c, way)) for way in range(2) if length(c, way)]
+        else:
+            settle(direct.at[c, pl.ds(0, ny - 1), :, filled], d_rs.at[c])
+            terms = [direct.at[c, k] for k in range(ny - 1)]
 
         def summed(t):
             total = part[c, y, t].astype(F32)
-            for k in range(ny - 1):
-                total += direct[c, k, t].astype(F32)
+            for term in terms:
+                total += term[t].astype(F32)
             return total * inverse
 
         for t in range(tiles):
@@ -234,10 +300,10 @@
             ).start()
         xr[x, c] = po[x, c]
 
-    def r_copy(s):
+    def r_copy(n):
         return pltpu.make_async_remote_copy(
-            src_ref=back.at[:, s, filled], dst_ref=ret.at[pl.ds(2 * ep, 2), filled],
-            send_sem=r_ss, recv_sem=r_rs, **on_z(s),
+            src_ref=back.at[:, n, filled], dst_ref=ret.at[pl.ds(2 * ep, 2), filled],
+            send_sem=r_ss, recv_sem=r_rs, **on_z(source_of(n)),
         )
 
     def give_back(c):
@@ -246,7 +312,7 @@
             back[e, c * ny : (c + 1) * ny] = (xr[2 * e, c].astype(F32) + xr[2 * e + 1, c].astype(F32)).astype(BF16)
 
         def r_start(i, carry):
-            @pl.when(c * ny + i != ep)
+            @pl.when(c * ny + i != mine)
             def _():
                 r_copy(c * ny + i).start()
 
@@ -255,7 +321,6 @@
         lax.fori_loop(0, ny, r_start, 0)
 
     def join_gate_up():
-        settle(wland.at[:, 0], l_sem)
         settle(gain_all.at[pl.ds(0, NX - 1)], g_rs)
         for n in range(2):
             settle(wland.at[n, pl.ds(0, NX - 1)], w_rs.at[n])
@@ -267,38 +332,73 @@
         for s in range(NX):
             wdn[:, s * feats : (s + 1) * feats] = wland[2, s]
 
-    ahead = min(2, chunks)
-    for c in range(ahead):
+    p_iota = lax.broadcasted_iota(jnp.int32, (toks, experts * PAD), 1).astype(F32)
+    for k in range(2):
+        picks[k * toks : (k + 1) * toks] = jnp.where(p_iota == tcol[:, k : k + 1], 1.0, 0.0).astype(BF16)
+    for c in range(min(3, chunks)):
         arrive(c)
     join_gate_up()
-    for c in range(ahead):
+    for c in range(chunks):
         gate_up(c)
-        if c + ahead < chunks:
-            arrive(c + ahead)
-    send_weight(2)
-    p_iota = lax.broadcasted_iota(jnp.int32, (toks, experts * PAD), 1).astype(F32)
-    for k in range(2):
-        picks[k] = jnp.where(p_iota == tcol[:, k : k + 1], 1.0, 0.0).astype(BF16)
-    for c in range(ahead):
-        activate(c)
-        if c + ahead < chunks:
-            gate_up(c + ahead)
-    join_down()
-    down(0)
-    for c in range(chunks):
-        if c + ahead < chunks:
-            activate(c + ahead)
-        if c + 1 < chunks:
-            down(c + 1)
-        give_back(c)
+        if c < straight:
+            send_sums(c)
+        else:
+
+            @pl.when(core == 1)
+            def _():
+                send_chain(c)
+
+        if c + 3 < chunks:
+            arrive(c + 3)
+        if c == straight - 1:
+            send_weight(2)
+
+    @pl.when(core == 0)
+    def _():
+        for c in range(straight):
+            activate(c)
+            send_sums(c + straight)
+        join_down()
+        down(0)
+        for c in range(chunks):
+            if c + straight < chunks:
+                activate(c + straight)
+            if c + 1 < chunks:
+                down(c + 1)
+            give_back(c)
+        settle(direct.at[:, :, :, filled], d_ss)
+
+    @pl.when(core == 1)
+    def _():
+        for c in range(straight):
+            activate(c)
+            if c + 2 <= longest:
+                hop(c + 2)
+        join_down()
+        down(0)
+        for s in range(straight + 2, longest + 1):
+            hop(s)
+        for c in range(1, straight):
+            down(c)
+        give_back(0)
+        for c in range(straight, chunks):
+            activate(c, True)
+        for c in range(1, straight):
+            give_back(c)
+        for c in range(straight, chunks):
+            down(c)
+        for c in range(straight, chunks):
+            give_back(c)
+        settle(direct.at[pl.ds(0, straight), :, :, filled], d_ss)
+        settle(chain.at[:, :, :, filled], y_ss)
+
     for e in range(2):
-        ret[2 * ep + e, 0:cap] = back[e, ep, 0:cap]
+        ret[2 * ep + e, 0:cap] = back[e, mine, 0:cap]
 
     settle(zsend.at[pl.ds(0, 2 * (n_ep - 1)), filled], z_ss)
     settle(gain_all.at[pl.ds(0, NX - 1)], g_ss)
     settle(wland.at[:, pl.ds(0, NX - 1)], w_ss)
     settle(xg.at[pl.ds(0, NX - 1), :, filled], x_ss)
-    settle(direct.at[:, :, :, filled], d_ss)
     settle(ssq_all, q_ss)
     settle(hid.at[:, pl.ds(0, ny - 1), :, filled], h_ss)
     settle(xr.at[pl.ds(0, NX - 1), :, :, filled], o_ss)
@@ -306,7 +406,8 @@
     everyone = ret.at[pl.ds(0, 2 * (n_ep - 1)), filled]
     settle(everyone, r_rs)
     answers = ret[...].reshape(experts * PAD, feats)
-    out_ref[...] = (dot_nn(picks[0], answers) * tcol[:, 2:3] + dot_nn(picks[1], answers) * tcol[:, 3:4]).astype(BF16)
+    picked = dot_nn(picks[...], answers)
+    out_ref[...] = (picked[:toks] * tcol[:, 2:3] + picked[toks:] * tcol[:, 3:4]).astype(BF16)
     settle(everyone, r_ss)
 
 
@@ -349,9 +450,12 @@
             pltpu.VMEM((2, n_ep, PAD, feats), BF16),
             pltpu.VMEM((experts, PAD, feats), BF16),
             pltpu.VMEM((toks, 128), F32),
-            pltpu.VMEM((2, toks, experts * PAD), BF16),
+            pltpu.VMEM((2 * toks, experts * PAD), BF16),
+            pltpu.VMEM((3, *w_gate.shape), BF16),
+            pltpu.VMEM((chunks - chunks // 2, ny - 1, 2 * tiles, PAD, 128), BF16),
+            pltpu.VMEM((chunks - chunks // 2, ny - 1, 2 * tiles, PAD, 128), BF16),
             dma, each, dma, dma, dma, dma((3,)), dma, dma, dma, each,
-            dma, each, dma, each, dma, each, dma, each, dma, dma((4,)),
+            dma, each, dma, each, dma, each, dma, each, dma, dma((4,)), dma, dma((chunks - chunks // 2, ny - 1)),
         ],
         compiler_params=pltpu.CompilerParams(collective_id=0, has_side_effects=True),
         name="routed_layer",

time: 64.4 us -> 63.5 us (0.986)
  the two profiles are of different devices: /device:TPU:8 before, /device:TPU:1 now
where the time goes in v4:
time: 63.5 us; the launch traced here: 62.3 us
  Pallas kernels  61.6 us (97%)
    pallas_call x1, Pallas kernels, layer(): pl.pallas_call(functools.partial(kernel, n_ep, ny, cap), out_shape=pltpu....  61.6 us

profile of v4, /device:TPU:1, one launch (start us, length us, event | category | flops | bytes accessed | tf_op | source)
XLA Modules:
  0.0 62.3 jit_solution(3330262286150262235)
XLA Ops:
  0.0 61.6 %routed_layer.1 = bf16[256,128]{1,0:T(8,128)(2,1)S(1)} custom-call(bf16[256,128]{1,0:T(8,128)(2,1)} %tok_hbm.1, f32[1,128]{1,0:T(1,128)} %bitcast.5, s32[2,256]{1,0:T(2,128)} %bitcast.3, f32[2,256]{1,0:T(2,128)} %bitcast.4, bf16[2,768,128]{2,1,0:T(8,128)(2,1)} %wg_ref.1, bf16[2,768,128]{2,1,0:T(8,128)(2,1)} %wu_ref.1, bf16[2,768,128]{2,1,0:T(8,128)(2,1)} %wd_ref.1), custom_call_target="tpu_custom_call" | custom-call | tf_op jit(solution)/shard_map/routed_layer/pallas_call | solution.py:425
  61.6 0.6 %copy.9 = bf16[256,128]{1,0:T(8,128)(2,1)} copy(bf16[256,128]{1,0:T(8,128)(2,1)S(1)} %routed_layer.1) | data formatting | bytes 131072

commit v5 on v4

--- a/solution.py
+++ b/solution.py
@@ -356,8 +356,8 @@
     @pl.when(core == 0)
     def _():
         for c in range(straight):
+            send_sums(c + straight)
             activate(c)
-            send_sums(c + straight)
         join_down()
         down(0)
         for c in range(chunks):

time: 63.5 us -> 63.2 us (level); the launches traced: 62.3 us -> 63 us
  Pallas kernels: 61.6 us -> 62.4 us
    pallas_call x1, Pallas kernels: 61.6 us -> 62.4 us  [layer(): pl.pallas_call(functools.partial(kernel, n_ep, ny, cap), out_shape=pltpu....]
where the time goes in v5:
time: 63.2 us; the launch traced here: 63 us
  Pallas kernels  62.4 us (99%)
    pallas_call x1, Pallas kernels, layer(): pl.pallas_call(functools.partial(kernel, n_ep, ny, cap), out_shape=pltpu....  62.4 us

profile of v5, /device:TPU:1, one launch (start us, length us, event | category | flops | bytes accessed | tf_op | source)
XLA Modules:
  0.0 63.0 jit_solution(4804731518853419529)
XLA Ops:
  0.0 62.4 %routed_layer.1 = bf16[256,128]{1,0:T(8,128)(2,1)S(1)} custom-call(bf16[256,128]{1,0:T(8,128)(2,1)} %tok_hbm.1, f32[1,128]{1,0:T(1,128)} %bitcast.5, s32[2,256]{1,0:T(2,128)} %bitcast.3, f32[2,256]{1,0:T(2,128)} %bitcast.4, bf16[2,768,128]{2,1,0:T(8,128)(2,1)} %wg_ref.1, bf16[2,768,128]{2,1,0:T(8,128)(2,1)} %wu_ref.1, bf16[2,768,128]{2,1,0:T(8,128)(2,1)} %wd_ref.1), custom_call_target="tpu_custom_call" | custom-call | tf_op jit(solution)/shard_map/routed_layer/pallas_call | solution.py:425
  62.4 0.6 %copy.9 = bf16[256,128]{1,0:T(8,128)(2,1)} copy(bf16[256,128]{1,0:T(8,128)(2,1)S(1)} %routed_layer.1) | data formatting | bytes 131072
